TPU v7x, 32 devices: a whole 2x2x4 slice. The times are simulated.
32 devices in a mesh: fs: 4 (over y, x), tp: 8 (over z, core).
Axes of the slice: x: 2, y: 2, z: 4, core: 2. Of those that a mesh axis runs over, the one named last changes fastest.
Arguments:
- tokens: bfloat16 [4096, 2048], P(('fs', 'tp')), may hold values from -6 to 6
- gain: float32 [2048], P('fs'), may hold values from 0.1 to 1.9
- ex_gate: float32 [8, 256, 2048], P('tp', None, 'fs'), may hold values from -0.125 to 0.125
- ex_up: float32 [8, 256, 2048], P('tp', None, 'fs'), may hold values from -0.125 to 0.125
- ex_down: float32 [8, 256, 2048], P('tp', None, 'fs'), may hold values from -0.375 to 0.375
- sh_gate: float32 [512, 2048], P('tp', 'fs'), may hold values from -0.125 to 0.125
- sh_up: float32 [512, 2048], P('tp', 'fs'), may hold values from -0.125 to 0.125
- sh_down: float32 [512, 2048], P('tp', 'fs'), may hold values from -0.25 to 0.25
- routes: int32 [4096, 4], P(('fs', 'tp')), may hold values from 0 to 7, all different within a row; in each aligned block of 128 rows (0 to 127, 128 to 255, ...) at most 72 rows name the same one
- route_weight: float32 [4096, 4], P(('fs', 'tp')), may hold values from 0.1 to 1
Outputs:
- mixed: bfloat16 [4096, 2048], P(('fs', 'tp'))
- expert_gate: bfloat16 [8, 256, 2048], P('tp')
- expert_up: bfloat16 [8, 256, 2048], P('tp')
- expert_down: bfloat16 [8, 256, 2048], P('tp')
- shared_gate: bfloat16 [512, 2048], P('tp')
- shared_up: bfloat16 [512, 2048], P('tp')
- shared_down: bfloat16 [512, 2048], P('tp')
Inputs may be any that keep to these rules, and one draw needn't show every extreme that they name: `routes`: each row names 4 different experts. Among the rows of one device no expert is named by more than 72 rows, and in every draw some expert is named by exactly 72 rows of some device.
All inputs are finite; a program needn't handle non-finite values.
Results may differ from a plain program's by a relative error of at most 0.0085.
Values may be sent and summed in bfloat16 or wider, within the bound.
A program may use at most 64 MiB of HBM per device.

v0:
```python
import jax
import jax.numpy as jnp
from jax import lax
from jax.sharding import PartitionSpec as P

EPS = 1e-06
ROUTED_SCALE = 2.5
CONTRACT = (((1,), (1,)), ((), ()))


def against(row_block, weight):
    return lax.dot_general(row_block, weight, CONTRACT, preferred_element_type=jnp.float32)


def hidden_of(row_block, w_gate, w_up):
    return (jax.nn.silu(against(row_block, w_gate)) * against(row_block, w_up)).astype(jnp.bfloat16)


def expert_apply(row_block, w_gate, w_up, w_down):
    return jnp.dot(hidden_of(row_block, w_gate, w_up), w_down, preferred_element_type=jnp.float32)


def slot_numbers(expert_ids, experts, capacity):
    flat_ids = expert_ids.reshape(-1)
    onehot = (flat_ids[:, None] == jnp.arange(experts, dtype=jnp.int32)[None, :]).astype(jnp.int32)
    before = jnp.cumsum(onehot, axis=0) - onehot
    ranking = jnp.sum(before * onehot, axis=1)
    return flat_ids * capacity + ranking


def local(tokens, gain, ex_gate, ex_up, ex_down, sh_gate, sh_up, sh_down, routes, route_weight):
    scale = gain[None, :]
    fold_gate = (ex_gate * scale[None]).astype(jnp.bfloat16)
    fold_up = (ex_up * scale[None]).astype(jnp.bfloat16)
    fold_down = ex_down.astype(jnp.bfloat16)
    fold_sgate = (sh_gate * scale).astype(jnp.bfloat16)[None]
    fold_sup = (sh_up * scale).astype(jnp.bfloat16)[None]
    fold_sdown = sh_down.astype(jnp.bfloat16)[None]
    tok_rows = tokens.shape[0]
    width = tokens.shape[1]
    top = routes.shape[1]
    experts = lax.axis_size("tp")
    capacity = tok_rows * top * 9 // (8 * experts)
    values = tokens.astype(jnp.float32)
    normed = (values * lax.rsqrt(jnp.mean(values * values, axis=1, keepdims=True) + EPS)).astype(
        jnp.bfloat16
    )
    weights = route_weight / jnp.sum(route_weight, axis=1, keepdims=True) * ROUTED_SCALE
    slots = slot_numbers(routes, experts, capacity)
    spots = jnp.arange(experts * capacity, dtype=jnp.int32)
    placing = (spots[:, None] == slots[None, :]).astype(jnp.int32)
    placing = jnp.sum(placing.reshape(experts * capacity, tok_rows, top), axis=2).astype(
        jnp.bfloat16
    )
    outgoing = jnp.dot(placing, normed, preferred_element_type=jnp.float32).astype(jnp.bfloat16)
    outgoing = outgoing.reshape(experts, capacity, width)
    whole = (
        lax.all_gather(fold_gate, "fs", axis=2, tiled=True),
        lax.all_gather(fold_up, "fs", axis=2, tiled=True),
        lax.all_gather(fold_down, "fs", axis=2, tiled=True),
        lax.all_gather(fold_sgate, "fs", axis=2, tiled=True),
        lax.all_gather(fold_sup, "fs", axis=2, tiled=True),
        lax.all_gather(fold_sdown, "fs", axis=2, tiled=True),
    )
    exp_gate, exp_up, exp_down = (whole[0], whole[1], whole[2])
    shr_gate, shr_up, shr_down = (whole[3][0], whole[4][0], whole[5][0])
    arrived = lax.all_to_all(outgoing, "tp", split_axis=0, concat_axis=0, tiled=True)
    sources = arrived.shape[0]
    count = arrived.shape[1]
    flat_rows = arrived.reshape(sources * count, width)
    result = expert_apply(flat_rows, exp_gate[0], exp_up[0], exp_down[0]).astype(jnp.bfloat16)
    answered = result.reshape(sources, count, width)
    returned = lax.all_to_all(answered, "tp", split_axis=0, concat_axis=0, tiled=True).reshape(
        experts * capacity, width
    )
    picked = returned[slots].reshape(tok_rows, top, width)
    routed = jnp.sum(weights[:, :, None] * picked.astype(jnp.float32), axis=1)
    shared = expert_apply(
        normed,
        lax.all_gather(shr_gate, "tp", axis=0, tiled=True),
        lax.all_gather(shr_up, "tp", axis=0, tiled=True),
        lax.all_gather(shr_down, "tp", axis=0, tiled=True),
    )
    mixed = (shared + routed).astype(jnp.bfloat16)
    return (mixed, exp_gate, exp_up, exp_down, shr_gate, shr_up, shr_down)


def solution(mesh):
    in_specs = (
        P(("fs", "tp"), None),
        P("fs"),
        P("tp", None, "fs"),
        P("tp", None, "fs"),
        P("tp", None, "fs"),
        P("tp", "fs"),
        P("tp", "fs"),
        P("tp", "fs"),
        P(("fs", "tp"), None),
        P(("fs", "tp"), None),
    )
    out_specs = (
        P(("fs", "tp"), None),
        P("tp", None, None),
        P("tp", None, None),
        P("tp", None, None),
        P("tp", None),
        P("tp", None),
        P("tp", None),
    )
    return jax.shard_map(local, mesh=mesh, in_specs=in_specs, out_specs=out_specs, check_vma=False)
```

profile of v0, /device:TPU:0, one launch (start us, length us, event | category | flops | bytes accessed | tf_op | source)
XLA Modules:
  0.0 238.6 jit_solution(3136089401162151272)
XLA Ops:
  7.3 2.2 multiply_convert_fusion.1
  9.6 0.7 all-gather.15.cloned.1.call-update
  10.3 0.7 convert_element_type.73
  11.2 11.2 %all-gather = bf16[64,2048]{1,0:T(8,128)(2,1)} all-gather(bf16[64,512]{1,0:T(8,128)(2,1)S(1)} %get-tuple-element.9), channel_id=2, replica_groups=mesh['fs'=4,'tp'=8] {'fs'}, dimensions={1}, use_global_device_ids=true | all-gather | bytes 327680 | tf_op jit(solution)/shard_map/all_gather | solution.py:61
  22.8 1.1 reduce-window.6
  23.9 0.2 slice_reduce_fusion
  24.4 0.2 convert_reduce_fusion
  24.6 0.2 fusion.3
  24.8 2.3 convolution_convert_fusion.1
  27.1 4.9 %all-to-all-start = ((bf16[8,72,2048]{2,1,0:T(8,128)(2,1)}), bf16[8,72,2048]{2,1,0:T(8,128)(2,1)S(1)}, u32[]{:S(2)}, u32[]{:S(2)}) async-start(bf16[8,72,2048]{2,1,0:T(8,128)(2,1)} %bitcast.2), calls=%async_computation | async-start | bytes 4718592 | tf_op jit(solution)/shard_map/all_to_all | solution.py:67
  32.0 10.6 %all-gather.2 = bf16[64,2048]{1,0:T(8,128)(2,1)} all-gather(bf16[64,512]{1,0:T(8,128)(2,1)S(1)} %get-tuple-element.10), channel_id=4, replica_groups=mesh['fs'=4,'tp'=8] {'fs'}, dimensions={1}, use_global_device_ids=true | all-gather | bytes 327680 | tf_op jit(solution)/shard_map/all_gather | solution.py:62
  42.7 44.0 %all-to-all-done = bf16[8,72,2048]{2,1,0:T(8,128)(2,1)S(1)} async-done(((bf16[8,72,2048]{2,1,0:T(8,128)(2,1)}), bf16[8,72,2048]{2,1,0:T(8,128)(2,1)S(1)}, u32[]{:S(2)}, u32[]{:S(2)}) %all-to-all-start) | async-done | bytes 2359328 | tf_op jit(solution)/shard_map/all_to_all | solution.py:67
  86.6 2.9 %fusion.8 = f32[576,256]{1,0:T(8,128)} fusion(bf16[576,2048]{1,0:T(8,128)(2,1)S(1)} %bitcast.31, bf16[1,256,2048]{2,1,0:T(8,128)(2,1)} %all-gather.13.cloned.1.call-done), kind=kOutput, calls=%fused_computation.18 | convolution fusion | flops 603979776 | bytes 3997696 | tf_op jit(solution)/shard_map/dot_general | solution.py:12
  89.5 8.4 %all-gather.17.cloned.1.call-done = bf16[1,256,2048]{2,1,0:T(8,128)(2,1)} async-done(((bf16[1,256,512]{2,1,0:T(8,128)(2,1)}), bf16[1,256,2048]{2,1,0:T(8,128)(2,1)}) %all-gather.17.cloned.1.call-update) | async-done | bytes 1048592 | tf_op jit(solution)/shard_map/all_gather | solution.py:60
  97.9 5.7 %convolution_convert_fusion = bf16[576,2048]{1,0:T(8,128)(2,1)} fusion(bf16[576,2048]{1,0:T(8,128)(2,1)S(1)} %bitcast.32, bf16[1,256,2048]{2,1,0:T(8,128)(2,1)} %all-gather.17.cloned.1.call-done, bf16[1,256,2048]{2,1,0:T(8,128)(2,1)} %all-gather.15.cloned.1.call-done, f32[576,256]{1,0:T(8,128)} %fusion.8), kind=kOutput, calls=%fused_computation.2 | convolution fusion | flops 1210023936 | bytes 7405568 | tf_op jit(solution)/shard_map/dot_general | solution.py:20
  103.6 4.7 %all-to-all-start.1 = ((bf16[8,72,2048]{2,1,0:T(8,128)(2,1)}), bf16[8,72,2048]{2,1,0:T(8,128)(2,1)S(1)}, u32[]{:S(2)}, u32[]{:S(2)}) async-start(bf16[8,72,2048]{2,1,0:T(8,128)(2,1)} %bitcast.30), calls=%async_computation.1 | async-start | bytes 4718592 | tf_op jit(solution)/shard_map/all_to_all | solution.py:73
  108.4 9.8 %all-gather.4 = bf16[64,2048]{1,0:T(8,128)(2,1)} all-gather(bf16[64,512]{1,0:T(8,128)(2,1)S(1)} %convert_element_type.64), channel_id=6, replica_groups=mesh['fs'=4,'tp'=8] {'fs'}, dimensions={1}, use_global_device_ids=true | all-gather | bytes 327680 | tf_op jit(solution)/shard_map/all_gather | solution.py:63
  118.5 25.1 %all-gather.19.cloned.1.call-done = bf16[512,2048]{1,0:T(8,128)(2,1)} async-done(((bf16[64,2048]{1,0:T(8,128)(2,1)}), bf16[512,2048]{1,0:T(8,128)(2,1)}) %all-gather.19.cloned.1.call-update) | async-done | bytes 2097168 | tf_op jit(solution)/shard_map/all_gather | solution.py:80
  143.6 2.4 %fusion.32 = f32[128,512]{1,0:T(8,128)S(1)} fusion(bf16[512,2048]{1,0:T(8,128)(2,1)} %all-gather.19.cloned.1.call-done, bf16[128,2048]{1,0:T(8,128)(2,1)S(1)} %copy-done, f32[128]{0:T(128)S(1)} %add_rsqrt_fusion), kind=kOutput, calls=%fused_computation.52 | convolution fusion | flops 269221888 | bytes 2884096 | tf_op jit(solution)/shard_map/dot_general | solution.py:12
  146.0 48.9 %all-to-all-done.1 = bf16[8,72,2048]{2,1,0:T(8,128)(2,1)S(1)} async-done(((bf16[8,72,2048]{2,1,0:T(8,128)(2,1)}), bf16[8,72,2048]{2,1,0:T(8,128)(2,1)S(1)}, u32[]{:S(2)}, u32[]{:S(2)}) %all-to-all-start.1) | async-done | bytes 2359328 | tf_op jit(solution)/shard_map/all_to_all | solution.py:73
  194.9 3.3 %gather_fusion = bf16[512,2048]{1,0:T(8,128)(2,1)} fusion(bf16[576,2048]{1,0:T(8,128)(2,1)S(1)} %bitcast.29, s32[1024]{0:T(1024)S(1)} %pad_clamp_fusion), kind=kCustom, calls=%fused_computation | custom fusion | bytes 4196352 | tf_op jit(solution)/shard_map/gather | solution.py:76
  198.2 4.9 %reshape.111 = f32[128,4,2048]{2,1,0:T(4,128)} reshape(bf16[512,2048]{1,0:T(8,128)(2,1)} %gather_fusion) | data formatting | bytes 6291456 | tf_op jit(solution)/shard_map/convert_element_type | solution.py:77
  203.0 5.4 %multiply_reduce_fusion = f32[128,2048]{1,0:T(8,128)S(1)} fusion(f32[128,4,2048]{2,1,0:T(4,128)} %reshape.111, f32[128,4]{1,0:T(8,128)S(1)} %copy.23), kind=kLoop, calls=%fused_computation.1 | loop fusion | flops 1835008 | bytes 5244928 | tf_op jit(solution)/shard_map/reduce_sum | solution.py:77
  208.5 13.4 %all-gather.23.cloned.1.call-done = bf16[512,2048]{1,0:T(8,128)(2,1)} async-done(((bf16[64,2048]{1,0:T(8,128)(2,1)}), bf16[512,2048]{1,0:T(8,128)(2,1)}) %all-gather.23.cloned.1.call-update) | async-done | bytes 2097168 | tf_op jit(solution)/shard_map/all_gather | solution.py:82
  221.8 4.3 %fusion = bf16[128,2048]{1,0:T(8,128)(2,1)} fusion(f32[128,2048]{1,0:T(8,128)S(1)} %multiply_reduce_fusion, bf16[512,2048]{1,0:T(8,128)(2,1)} %all-gather.23.cloned.1.call-done, bf16[512,2048]{1,0:T(8,128)(2,1)} %all-gather.21.cloned.1.call-done, f32[128,512]{1,0:T(8,128)S(1)} %fusion.32, bf16[128,2048]{1,0:T(8,128)(2,1)S(1)} %copy-done, ...), kind=kOutput, calls=%fused_computation.5 | convolution fusion | flops 538574848 | bytes 6554112 | tf_op jit(solution)/shard_map/dot_general | solution.py:20
  226.1 1.0 copy.34
  227.0 0.6 copy-done.5
  227.7 1.0 copy.35
  228.6 1.0 copy.36
  229.6 0.7 copy.37
  230.3 0.7 copy.38
  231.0 0.7 copy.39
  (60 shorter events, 1.4 us)
Async XLA Ops:
  7.2 4.0 %copy-start.11 = (f32[512]{0:T(512)S(1)}, f32[512]{0:T(512)}, u32[]{:S(2)}) copy-start(f32[512]{0:T(512)} %param.11) | copy-start | bytes 6148
  7.2 3.1 %copy-start.7 = (f32[1,256,512]{2,1,0:T(8,128)S(1)}, f32[1,256,512]{2,1,0:T(8,128)}, u32[]{:S(2)}) copy-start(f32[1,256,512]{2,1,0:T(8,128)} %param.14) | copy-start | bytes 1572868
  7.2 4.0 %copy-start.8 = (f32[64,512]{1,0:T(8,128)S(1)}, f32[64,512]{1,0:T(8,128)}, u32[]{:S(2)}) copy-start(f32[64,512]{1,0:T(8,128)} %param.15) | copy-start | bytes 393220
  7.2 4.0 %copy-start.9 = (f32[64,512]{1,0:T(8,128)S(1)}, f32[64,512]{1,0:T(8,128)}, u32[]{:S(2)}) copy-start(f32[64,512]{1,0:T(8,128)} %param.16) | copy-start | bytes 393220
  7.2 15.2 %copy-start.13 = (s32[128,4]{0,1:T(4,128)S(1)}, s32[128,4]{0,1:T(4,128)}, u32[]{:S(2)}) copy-start(s32[128,4]{0,1:T(4,128)} %param.18) | copy-start | bytes 6148
  7.2 17.4 %copy-start = (bf16[128,2048]{1,0:T(8,128)(2,1)S(1)}, bf16[128,2048]{1,0:T(8,128)(2,1)}, u32[]{:S(2)}) copy-start(bf16[128,2048]{1,0:T(8,128)(2,1)} %param.10) | copy-start | bytes 1572868
  7.2 35.4 %all-gather.13.cloned.1.call-start = ((), (), s32[]{:S(2)}) async-start(), calls=%async_computation.2 | async-start | bytes 1310720 | tf_op jit(solution)/shard_map/all_gather | solution.py:58
  9.5 80.0 %all-gather.15.cloned.1.call-start = ((), (), s32[]{:S(2)}) async-start(), calls=%async_computation.3 | async-start | bytes 1310720 | tf_op jit(solution)/shard_map/all_gather | solution.py:59
  10.3 87.6 %all-gather.17.cloned.1.call-start = ((), (), s32[]{:S(2)}) async-start(), calls=%async_computation.4 | async-start | bytes 1310720 | tf_op jit(solution)/shard_map/all_gather | solution.py:60
  11.1 132.5 %all-gather.19.cloned.1.call-start = ((), (), s32[]{:S(2)}) async-start(), calls=%async_computation.5 | async-start | bytes 2359296 | tf_op jit(solution)/shard_map/all_gather | solution.py:80
  27.1 59.5 %all-to-all-start = ((bf16[8,72,2048]{2,1,0:T(8,128)(2,1)}), bf16[8,72,2048]{2,1,0:T(8,128)(2,1)S(1)}, u32[]{:S(2)}, u32[]{:S(2)}) async-start(bf16[8,72,2048]{2,1,0:T(8,128)(2,1)} %bitcast.2), calls=%async_computation | async-start | bytes 4718592 | tf_op jit(solution)/shard_map/all_to_all | solution.py:67
  32.0 176.5 %all-gather.21.cloned.1.call-start = ((), (), s32[]{:S(2)}) async-start(), calls=%async_computation.6 | async-start | bytes 2359296 | tf_op jit(solution)/shard_map/all_gather | solution.py:81
  103.6 4.8 %copy-start.10 = (f32[64,512]{1,0:T(8,128)S(1)}, f32[64,512]{1,0:T(8,128)}, u32[]{:S(2)}) copy-start(f32[64,512]{1,0:T(8,128)} %param.17) | copy-start | bytes 393220
  103.6 14.7 %copy-start.12 = (f32[128,4]{0,1:T(4,128)S(1)}, f32[128,4]{0,1:T(4,128)}, u32[]{:S(2)}) copy-start(f32[128,4]{0,1:T(4,128)} %param.19) | copy-start | bytes 6148
  103.6 91.2 %all-to-all-start.1 = ((bf16[8,72,2048]{2,1,0:T(8,128)(2,1)}), bf16[8,72,2048]{2,1,0:T(8,128)(2,1)S(1)}, u32[]{:S(2)}, u32[]{:S(2)}) async-start(bf16[8,72,2048]{2,1,0:T(8,128)(2,1)} %bitcast.30), calls=%async_computation.1 | async-start | bytes 4718592 | tf_op jit(solution)/shard_map/all_to_all | solution.py:73
  108.4 113.5 %all-gather.23.cloned.1.call-start = ((), (), s32[]{:S(2)}) async-start(), calls=%async_computation.7 | async-start | bytes 2359296 | tf_op jit(solution)/shard_map/all_gather | solution.py:82
  208.4 17.7 %copy-start.4 = (bf16[1,256,2048]{2,1,0:T(8,128)(2,1)S(1)}, bf16[1,256,2048]{2,1,0:T(8,128)(2,1)}, u32[]{:S(2)}) copy-start(bf16[1,256,2048]{2,1,0:T(8,128)(2,1)} %all-gather.13.cloned.1.call-done) | copy-start | bytes 3145732
  226.1 1.6 copy-start.5
  226.1 2.6 %copy-start.6 = (bf16[1,256,2048]{2,1,0:T(8,128)(2,1)S(1)}, bf16[1,256,2048]{2,1,0:T(8,128)(2,1)}, u32[]{:S(2)}) copy-start(bf16[1,256,2048]{2,1,0:T(8,128)(2,1)} %all-gather.17.cloned.1.call-done) | copy-start | bytes 3145732
  227.7 2.0 copy-start.1
  227.7 2.7 %copy-start.2 = (bf16[64,2048]{1,0:T(8,128)(2,1)S(1)}, bf16[64,2048]{1,0:T(8,128)(2,1)}, u32[]{:S(2)}) copy-start(bf16[64,2048]{1,0:T(8,128)(2,1)} %all-gather.2) | copy-start | bytes 786436
  227.7 3.4 %copy-start.3 = (bf16[64,2048]{1,0:T(8,128)(2,1)S(1)}, bf16[64,2048]{1,0:T(8,128)(2,1)}, u32[]{:S(2)}) copy-start(bf16[64,2048]{1,0:T(8,128)(2,1)} %all-gather.4) | copy-start | bytes 786436
Sparse Core Ops, SparseCore 0:
  10.4 29.7 all-gather.12
  42.7 26.3 all-gather.14
  71.5 26.3 all-gather.16
  99.3 44.2 all-gather.18
  145.0 47.8 all-gather.20
  194.4 27.3 all-gather.22
where the time goes:
time: 239 us
  waiting for transfers between devices  140 us (59%)
  blocking collectives  31.5 us (13%)
  matrix products  17.5 us (7%)
  local copies, waits for them, and re-layouts  14.8 us (6%)
  between operations  14.4 us (6%)
  other arithmetic  10 us (4%)
  starting transfers between devices  9.85 us (4%)
    all_to_all x1, waiting for transfers between devices, local(): lax.all_to_all(answered, 'tp', split_axis=0, concat_axis=0, tiled=True)  48.9 us
    all_to_all x1, waiting for transfers between devices, local(): lax.all_to_all(outgoing, 'tp', split_axis=0, concat_axis=0, tiled=True)  44 us
    all_gather x1, waiting for transfers between devices, local(): lax.all_gather(shr_gate, 'tp', axis=0, tiled=True)  25.1 us
    all_gather x1, waiting for transfers between devices, local(): lax.all_gather(shr_down, 'tp', axis=0, tiled=True)  13.4 us
    all_gather x1, blocking collectives, local(): lax.all_gather(fold_sgate, 'fs', axis=2, tiled=True)  11.2 us
    all_gather x1, blocking collectives, local(): lax.all_gather(fold_sup, 'fs', axis=2, tiled=True)  10.6 us
    dot_general x2, matrix products, expert_apply(): jnp.dot(hidden_of(row_block, w_gate, w_up), w_down, preferred_element_typ...  10 us
    all_gather x1, blocking collectives, local(): lax.all_gather(fold_sdown, 'fs', axis=2, tiled=True)  9.75 us
  transfers between devices with their start and end apart: 8, of which 5 were waited for; matrix products, arithmetic and copies ran while one was open for 13% of the time, Pallas kernels for 0%

commit v1 on v0

v1 whole, which is shorter than its diff:
```python
import functools

import jax
import jax.numpy as jnp
from jax import lax
from jax.experimental import pallas as pl
from jax.experimental.pallas import tpu as pltpu
from jax.sharding import PartitionSpec as P

EPS = 1e-06
ROUTED_SCALE = 2.5
CONTRACT = (((1,), (1,)), ((), ()))
MESH = pl.DeviceIdType.MESH
LAG = 2
RING = 16


def kernel(
    F, T, H, S, M,
    tokens, gain, ex_gate, ex_up, ex_down, sh_gate, sh_up, sh_down, routes, rweight,
    o_mixed, o_eg, o_eu, o_ed, o_sg, o_su, o_sd,
    tok, wbuf, wt, hid_e, hid_s, own, pout, pin, sout, sin, mix,
    ag_send, ag_recv, wt_send, wt_recv, w_send, w_recv,
    pout_sem, pin_sem, sout_sem, sin_sem, out_sem, mix_sem,
):
    f = lax.axis_index("fs")
    me = lax.axis_index("tp")
    z = me // 2
    c = lax.rem(me, 2)
    Z = T // 2
    cw = wbuf.shape[2]
    rows = tokens.shape[0]
    GU = 2 * H + 2 * S
    ALL = 3 * H + 3 * S
    partner = 2 * z + 1 - c

    barrier = pltpu.get_barrier_semaphore()
    for i in range(1, F):
        pl.semaphore_signal(barrier, inc=1, device_id=(lax.rem(f + i, F), me), device_id_type=MESH)
    for i in range(1, T):
        pl.semaphore_signal(barrier, inc=1, device_id=(f, lax.rem(me + i, T)), device_id_type=MESH)

    scale = gain[...]
    values = tokens[...].astype(jnp.float32)
    inv = lax.rsqrt(jnp.mean(values * values, axis=1, keepdims=True) + EPS)
    tok[me] = (values * inv).astype(jnp.bfloat16)
    wbuf[f, 0:H, :] = (ex_gate[...] * scale).astype(jnp.bfloat16)
    wbuf[f, H:2 * H, :] = (ex_up[...] * scale).astype(jnp.bfloat16)
    wbuf[f, 2 * H:2 * H + S, :] = (sh_gate[...] * scale).astype(jnp.bfloat16)
    wbuf[f, 2 * H + S:GU, :] = (sh_up[...] * scale).astype(jnp.bfloat16)
    wbuf[f, GU:GU + H, :] = ex_down[...].astype(jnp.bfloat16)
    wbuf[f, GU + H:ALL, :] = sh_down[...].astype(jnp.bfloat16)
    rw = rweight[...]
    w = rw / jnp.sum(rw, axis=1, keepdims=True) * ROUTED_SCALE
    ids = routes[...]
    lane = lax.broadcasted_iota(jnp.int32, (rows, 128), 1)
    comb = jnp.zeros((rows, 128), jnp.float32)
    for k in range(ids.shape[1]):
        comb = comb + jnp.where(lane == ids[:, k:k + 1], w[:, k:k + 1], 0.0)
    wt[me] = jnp.transpose(comb)[:T, :]

    pl.semaphore_wait(barrier, F - 1 + T - 1)

    def rdma(src, dst, ssem, rsem, dev):
        return pltpu.make_async_remote_copy(
            src_ref=src, dst_ref=dst, send_sem=ssem, recv_sem=rsem,
            device_id=dev, device_id_type=MESH,
        )

    def tok_copy(s, way, t):
        return rdma(tok.at[s], tok.at[s], ag_send.at[s, way], ag_recv.at[s], (f, t))

    def w_copy(part, src, i, peer):
        lo, hi = ((0, GU), (GU, ALL))[part]
        return rdma(
            wbuf.at[src, lo:hi, :], wbuf.at[src, lo:hi, :],
            w_send.at[part, i], w_recv.at[part, src], (peer, me),
        )

    def wt_copy(s, i, t):
        return rdma(wt.at[s], wt.at[s], wt_send.at[i], wt_recv.at[s], (f, t))

    def right(t):
        return jnp.minimum(t + 2, T - 2 + lax.rem(t, 2))

    def left(t):
        return jnp.maximum(t - 2, lax.rem(t, 2))

    @pl.when(z < Z - 1)
    def _():
        tok_copy(me, 0, right(me)).start()

    @pl.when(z > 0)
    def _():
        tok_copy(me, 1, left(me)).start()

    for i in range(1, F):
        w_copy(0, f, i, lax.rem(f + i, F)).start()
    tok_copy(me, 2, partner).start()
    for i in range(1, T):
        wt_copy(me, i, lax.rem(me + i, T)).start()
    for i in range(1, F):
        w_copy(1, f, i, lax.rem(f + i, F)).start()

    def gather_step(k, carry):
        a = me - 2 * k
        b = me + 2 * k

        @pl.when(a >= 0)
        def _():
            tok_copy(a, 0, partner).wait_recv()

            @pl.when(z < Z - 1)
            def _():
                tok_copy(a, 0, right(me)).start()

            tok_copy(a, 2, partner).start()

        @pl.when(b < T)
        def _():
            tok_copy(b, 1, partner).wait_recv()

            @pl.when(z > 0)
            def _():
                tok_copy(b, 1, left(me)).start()

            tok_copy(b, 2, partner).start()

        return carry

    lax.fori_loop(1, Z, gather_step, 0)

    for i in range(1, F):
        w_copy(0, lax.rem(f + F - i, F), i, f).wait_recv()
    for i in range(1, T):
        wt_copy(lax.rem(me + T - i, T), i, me).wait_recv()

    pieces = ((o_eg, 0, H), (o_eu, H, H), (o_sg, 2 * H, S), (o_su, 2 * H + S, S), (o_ed, GU, H), (o_sd, GU + H, S))

    def out_copy(p, q):
        ref, lo, size = pieces[p]
        return pltpu.make_async_copy(
            wbuf.at[q, lo:lo + size, :], ref.at[:, q * cw:(q + 1) * cw], out_sem.at[p, q]
        )

    for p in range(4):
        for q in range(F):
            out_copy(p, q).start()

    def hidden_step(k, carry):
        tok_copy(2 * k + 1 - c, 0, partner).wait_recv()
        x = tok[pl.ds(2 * k, 2)].reshape(2 * rows, F * cw)
        acc = jnp.zeros((2 * rows, GU), jnp.float32)
        for q in range(F):
            acc = acc + lax.dot_general(
                x[:, q * cw:(q + 1) * cw], wbuf[q, 0:GU, :], CONTRACT,
                preferred_element_type=jnp.float32,
            )
        g, u = acc[:, 0:H], acc[:, H:2 * H]
        sg, su = acc[:, 2 * H:2 * H + S], acc[:, 2 * H + S:GU]
        he = g / (1.0 + jnp.exp(-g)) * u
        hs = sg / (1.0 + jnp.exp(-sg)) * su
        for h in range(2):
            row = wt[2 * k + h, pl.ds(me, 1), :]
            col = jnp.transpose(jnp.broadcast_to(row, (128, rows)))[:, 0:1]
            hid_e[2 * k + h] = (he[h * rows:(h + 1) * rows] * col).astype(jnp.bfloat16)
            hid_s[2 * k + h] = hs[h * rows:(h + 1) * rows].astype(jnp.bfloat16)
        return carry

    lax.fori_loop(0, Z, hidden_step, 0)

    N = (Z - 1) * F
    U = Z * F
    ring = pout.shape[0]
    spot = jnp.where(2 * z >= Z, 2 * (Z - 1 - z), 2 * z + 1)

    def unit(u):
        i = lax.rem(u, Z - 1)
        i = i + jnp.where(i >= spot, 1, 0)
        d = jnp.where(lax.rem(i, 2) == 0, Z - 1 - i // 2, i // 2)
        j = u // (Z - 1)
        d = jnp.where(u < N, d, z)
        j = jnp.where(u < N, j, u - N)
        return j, d

    def pair_copy(u):
        p = lax.rem(u, ring)
        return rdma(pout.at[p], pin.at[u], pout_sem.at[p], pin_sem.at[u], (f, partner))

    def sum_copy(u, slot, t):
        p = lax.rem(u, ring)
        return rdma(sout.at[p], sin.at[slot], sout_sem.at[p], sin_sem.at[slot], (f, t))

    def mix_copy(q):
        return pltpu.make_async_copy(
            mix.at[q], o_mixed.at[:, pl.ds(pl.multiple_of(q * cw, 128), cw)], mix_sem.at[q]
        )

    def produce(u):
        j, d = unit(u)
        q = lax.rem(f + j, F)

        @pl.when((j > 0) & (lax.rem(u, Z - 1) == 0) & (u < N))
        def _():
            w_copy(1, q, 1, f).wait_recv()

        he = hid_e[pl.ds(2 * d, 2)].reshape(2 * rows, H)
        hs = hid_s[pl.ds(2 * d, 2)].reshape(2 * rows, S)
        r = jnp.dot(he, wbuf[q, GU:GU + H, :], preferred_element_type=jnp.float32)
        r = r + jnp.dot(hs, wbuf[q, GU + H:ALL, :], preferred_element_type=jnp.float32)
        top, bottom = r[:rows], r[rows:]
        own[lax.rem(u, LAG + 1)] = jnp.where(c == 0, top, bottom)

        @pl.when(u >= ring)
        def _():
            pair_copy(u - ring).wait_send()

        pout[lax.rem(u, ring)] = jnp.where(c == 0, bottom, top).astype(jnp.bfloat16)
        pair_copy(u).start()

    def finish(u):
        j, d = unit(u)
        q = lax.rem(f + j, F)
        o = lax.rem(u, LAG + 1)
        from_left = (d >= z) & (z > 0)
        from_right = (d <= z) & (z < Z - 1)
        pair_copy(u).wait_recv()
        own[o] = own[o] + pin[u].astype(jnp.float32)
        base = j * (Z + 1)

        @pl.when(from_left)
        def _():
            sum_copy(u, base + d, me).wait_recv()
            own[o] = own[o] + sin[base + d].astype(jnp.float32)

        @pl.when(from_right)
        def _():
            slot = base + jnp.where(d == z, Z, d)
            sum_copy(u, slot, me).wait_recv()
            own[o] = own[o] + sin[slot].astype(jnp.float32)

        @pl.when(u < N)
        def _():
            @pl.when(u >= ring)
            def _():
                sum_copy(u - ring, 0, partner).wait_send()

            sout[lax.rem(u, ring)] = own[o].astype(jnp.bfloat16)

            @pl.when(d > z)
            def _():
                sum_copy(u, base + d, right(me)).start()

            @pl.when(d < z)
            def _():
                sum_copy(u, base + jnp.where(d == z - 1, Z, d), left(me)).start()

        @pl.when(u >= N)
        def _():
            mix[q] = own[o].astype(jnp.bfloat16)
            mix_copy(q).start()

    def sum_step(u, carry):
        @pl.when(u < U)
        def _():
            produce(u)

        @pl.when(u >= LAG)
        def _():
            finish(u - LAG)

        return carry

    lax.fori_loop(0, U + LAG, sum_step, 0)

    for p in range(4, 6):
        for q in range(F):
            out_copy(p, q).start()
    for u in range(max(0, U - ring), U):
        pair_copy(u).wait_send()
    for u in range(max(0, N - ring), N):
        sum_copy(u, 0, partner).wait_send()
    for i in range(1, F):
        w_copy(0, f, i, lax.rem(f + i, F)).wait_send()
        w_copy(1, f, i, lax.rem(f + i, F)).wait_send()
    for i in range(1, T):
        wt_copy(me, i, lax.rem(me + i, T)).wait_send()

    def drain(k, carry):
        s = 2 * k + c

        @pl.when((k <= z) & (z < Z - 1))
        def _():
            tok_copy(s, 0, right(me)).wait_send()

        @pl.when((k >= z) & (z > 0))
        def _():
            tok_copy(s, 1, left(me)).wait_send()

        tok_copy(s, 2, partner).wait_send()
        return carry

    lax.fori_loop(0, Z, drain, 0)
    for q in range(F):
        mix_copy(q).wait()
    for p in range(6):
        for q in range(F):
            out_copy(p, q).wait()


def local(F, T, tokens, gain, ex_gate, ex_up, ex_down, sh_gate, sh_up, sh_down, routes, route_weight):
    H, cw = ex_gate.shape[1:]
    S = sh_gate.shape[0]
    M = tokens.shape[0]
    D = tokens.shape[1]
    Z = T // 2
    N, U = (Z - 1) * F, Z * F
    ring = min(U, RING)
    bf, f32 = jnp.bfloat16, jnp.float32
    dma = pltpu.SemaphoreType.DMA
    out = pl.pallas_call(
        functools.partial(kernel, F, T, H, S, M),
        out_shape=[jax.ShapeDtypeStruct((M, D), bf)]
        + [jax.ShapeDtypeStruct((H, D), bf)] * 3
        + [jax.ShapeDtypeStruct((S, D), bf)] * 3,
        in_specs=[pl.BlockSpec(memory_space=pltpu.VMEM)] * 10,
        out_specs=[pl.BlockSpec(memory_space=pl.ANY)] * 7,
        scratch_shapes=[
            pltpu.VMEM((T, M, D), bf),
            pltpu.VMEM((F, 3 * H + 3 * S, cw), bf),
            pltpu.VMEM((T, T, M), f32),
            pltpu.VMEM((T, M, H), bf),
            pltpu.VMEM((T, M, S), bf),
            pltpu.VMEM((LAG + 1, M, cw), f32),
            pltpu.VMEM((ring, M, cw), bf),
            pltpu.VMEM((U, M, cw), bf),
            pltpu.VMEM((ring, M, cw), bf),
            pltpu.VMEM((F * (Z + 1), M, cw), bf),
            pltpu.VMEM((F, M, cw), bf),
            dma((T, 3)),
            dma((T,)),
            dma((T,)),
            dma((T,)),
            dma((2, F)),
            dma((2, F)),
            dma((ring,)),
            dma((U,)),
            dma((ring,)),
            dma((F * (Z + 1),)),
            dma((6, F)),
            dma((F,)),
        ],
        compiler_params=pltpu.CompilerParams(
            collective_id=0, has_side_effects=True, vmem_limit_bytes=67043328
        ),
    )(
        tokens, gain[None, :], ex_gate[0], ex_up[0], ex_down[0], sh_gate, sh_up, sh_down,
        routes, route_weight,
    )
    mixed, eg, eu, ed, sg, su, sd = out
    return (mixed, eg[None], eu[None], ed[None], sg, su, sd)


def solution(mesh):
    in_specs = (
        P(("fs", "tp"), None),
        P("fs"),
        P("tp", None, "fs"),
        P("tp", None, "fs"),
        P("tp", None, "fs"),
        P("tp", "fs"),
        P("tp", "fs"),
        P("tp", "fs"),
        P(("fs", "tp"), None),
        P(("fs", "tp"), None),
    )
    out_specs = (
        P(("fs", "tp"), None),
        P("tp", None, None),
        P("tp", None, None),
        P("tp", None, None),
        P("tp", None),
        P("tp", None),
        P("tp", None),
    )
    step = functools.partial(local, mesh.shape["fs"], mesh.shape["tp"])
    return jax.shard_map(step, mesh=mesh, in_specs=in_specs, out_specs=out_specs, check_vma=False)
```

time: 239 us -> 115 us (0.48)
  waiting for transfers between devices: 140 us -> 0 us
  Pallas kernels: 0 us -> 102 us
  blocking collectives: 31.5 us -> 0 us
  matrix products: 17.5 us -> 0 us
  between operations: 14.4 us -> 0.67 us
  other arithmetic: 10 us -> 0 us
  starting transfers between devices: 9.85 us -> 0 us
  local copies, waits for them, and re-layouts: 14.8 us -> 11.2 us
    pallas_call x0 -> x1, Pallas kernels: none -> 102 us  [local(): pl.pallas_call(functools.partial(kernel, F, T, H, S, M), out_shape=[jax.S...]
    all_to_all x2 -> x0, waiting for transfers between devices: 92.8 us -> none  [the longest x1 48.9 us: local(): lax.all_to_all(answered, 'tp', split_axis=0, concat_axis=0, tiled=True)]
    all_gather x6 -> x0, waiting for transfers between devices: 46.9 us -> none  [the longest x1 25.1 us: local(): lax.all_gather(shr_gate, 'tp', axis=0, tiled=True)]
    all_gather x3 -> x0, blocking collectives: 31.5 us -> none  [the longest x1 11.2 us: local(): lax.all_gather(fold_sgate, 'fs', axis=2, tiled=True)]
    dot_general x5 -> x0, matrix products: 17.5 us -> none  [the longest x2 10 us: expert_apply(): jnp.dot(hidden_of(row_block, w_gate, w_up), w_down, preferred_element_typ...]
    all_to_all x2 -> x0, starting transfers between devices: 9.62 us -> none  [the longest x1 4.88 us: local(): lax.all_to_all(outgoing, 'tp', split_axis=0, concat_axis=0, tiled=True)]
    reduce_sum x5 -> x0, other arithmetic: 5.82 us -> none  [the longest x1 5.37 us: local(): routed = jnp.sum(weights[:, :, None] * picked.astype(jnp.float32), axis=1)]
    unnamed x35 -> x25, local copies, waits for them, and re-layouts: 5.81 us -> 11.2 us
  transfers between devices with their start and end apart: 8 -> 0, of which waited for: 5 -> 0; matrix products, arithmetic and copies ran while one was open for 13% -> 0% of each run, Pallas kernels for 0% -> 0%
where the time goes in v1:
time: 115 us; the launch traced here: 114 us
  Pallas kernels  102 us (89%)
  local copies, waits for them, and re-layouts  11.2 us (10%)
    pallas_call x1, Pallas kernels, local(): pl.pallas_call(functools.partial(kernel, F, T, H, S, M), out_shape=[jax.S...  102 us
    unnamed x25, local copies, waits for them, and re-layouts  11.2 us

profile of v1, /device:TPU:0, one launch (start us, length us, event | category | flops | bytes accessed | tf_op | source)
XLA Modules:
  0.0 114.2 jit_solution(10749455614355110999)
XLA Ops:
  0.6 0.0 copy-start.6
  0.6 0.7 copy-done.6
  1.3 0.0 copy-start.7
  1.3 0.7 copy.17.routes
  2.1 0.0 copy-done.7
  2.1 0.7 copy.18.rweight
  2.8 102.3 %shard_map.153 = (bf16[128,2048]{1,0:T(8,128)(2,1)}, bf16[256,2048]{1,0:T(8,128)(2,1)}, bf16[256,2048]{1,0:T(8,128)(2,1)}, bf16[256,2048]{1,0:T(8,128)(2,1)}, bf...) custom-call(bf16[128,2048]{1,0:T(8,128)(2,1)} %tokens.1, f32[1,512]{1,0:T(1,128)} %bitcast.13, ...), custom_call_target="tpu_custom_call" | custom-call | tf_op jit(solution)/shard_map/pallas_call | solution.py:321
  105.1 0.0 copy-start.2
  105.1 2.0 %copy.26 = bf16[128,2048]{1,0:T(8,128)(2,1)} copy(bf16[128,2048]{1,0:T(8,128)(2,1)} %get-tuple-element.28) | data formatting | bytes 1048576
  107.1 0.0 copy-done.2
  107.1 0.0 copy-start.1
  107.1 1.0 copy.27
  108.1 0.6 copy-done.1
  108.7 0.0 copy-start
  108.7 1.0 copy.28
  109.7 0.6 copy-done
  110.3 0.0 copy-start.5
  110.3 1.0 copy.29
  111.3 0.1 copy-done.5
  111.4 0.0 copy-start.4
  111.4 0.7 copy.30
  112.1 0.3 copy-done.4
  112.5 0.0 copy-start.3
  112.5 0.7 copy.31
  113.2 0.3 copy-done.3
  113.5 0.7 copy.32
Async XLA Ops:
  0.6 0.7 copy-start.6
  1.3 0.7 copy-start.7
  105.1 2.0 %copy-start.2 = (bf16[256,2048]{1,0:T(8,128)(2,1)S(1)}, bf16[256,2048]{1,0:T(8,128)(2,1)}, u32[]{:S(2)}) copy-start(bf16[256,2048]{1,0:T(8,128)(2,1)} %get-tuple-element.15) | copy-start | bytes 3145732
  107.1 1.6 %copy-start.1 = (bf16[256,2048]{1,0:T(8,128)(2,1)S(1)}, bf16[256,2048]{1,0:T(8,128)(2,1)}, u32[]{:S(2)}) copy-start(bf16[256,2048]{1,0:T(8,128)(2,1)} %get-tuple-element.16) | copy-start | bytes 3145732
  108.7 1.6 %copy-start = (bf16[256,2048]{1,0:T(8,128)(2,1)S(1)}, bf16[256,2048]{1,0:T(8,128)(2,1)}, u32[]{:S(2)}) copy-start(bf16[256,2048]{1,0:T(8,128)(2,1)} %get-tuple-element.17) | copy-start | bytes 3145732
  110.3 1.1 copy-start.5
  111.4 1.0 copy-start.4
  112.5 1.0 copy-start.3

commit v2 on v1

v2 whole, which is shorter than its diff:
```python
import functools

import jax
import jax.numpy as jnp
from jax import lax
from jax.experimental import pallas as pl
from jax.experimental.pallas import tpu as pltpu
from jax.sharding import PartitionSpec as P

EPS = 1e-06
ROUTED_SCALE = 2.5
CONTRACT = (((1,), (1,)), ((), ()))
MESH = pl.DeviceIdType.MESH
LAG = 2
RING = 16
VMEM_LIMIT = 56 << 20


def kernel(
    F, T, H, S, M,
    tokens, gain, ex_gate, ex_up, ex_down, sh_gate, sh_up, sh_down, routes, rweight,
    wbuf, mix,
    tok, wt, hid_e, hid_s, own, pout, pin, sout, sin,
    ag_send, ag_recv, wt_send, wt_recv, w_send, w_recv,
    pout_sem, pin_sem, sout_sem, sin_sem,
):
    f = lax.axis_index("fs")
    me = lax.axis_index("tp")
    z = me // 2
    c = lax.rem(me, 2)
    Z = T // 2
    cw = wbuf.shape[2]
    rows = tokens.shape[0]
    GU = 2 * H + 2 * S
    ALL = 3 * H + 3 * S
    partner = 2 * z + 1 - c

    barrier = pltpu.get_barrier_semaphore()
    for i in range(1, F):
        pl.semaphore_signal(barrier, inc=1, device_id=(lax.rem(f + i, F), me), device_id_type=MESH)
    for i in range(1, T):
        pl.semaphore_signal(barrier, inc=1, device_id=(f, lax.rem(me + i, T)), device_id_type=MESH)

    values = tokens[...].astype(jnp.float32)
    inv = lax.rsqrt(jnp.mean(values * values, axis=1, keepdims=True) + EPS)
    tok[me] = (values * inv).astype(jnp.bfloat16)
    rw = rweight[...]
    w = rw / jnp.sum(rw, axis=0, keepdims=True) * ROUTED_SCALE
    ids = routes[...]
    expert = lax.broadcasted_iota(jnp.int32, (T, rows), 0)
    comb = jnp.zeros((T, rows), jnp.float32)
    for k in range(ids.shape[0]):
        comb = comb + jnp.where(expert == ids[k:k + 1, :], w[k:k + 1, :], 0.0)
    wt[me] = comb

    pl.semaphore_wait(barrier, F - 1 + T - 1)

    def rdma(src, dst, ssem, rsem, dev):
        return pltpu.make_async_remote_copy(
            src_ref=src, dst_ref=dst, send_sem=ssem, recv_sem=rsem,
            device_id=dev, device_id_type=MESH,
        )

    def tok_copy(s, way, t):
        return rdma(tok.at[s], tok.at[s], ag_send.at[s, way], ag_recv.at[s], (f, t))

    def w_copy(part, src, i, peer):
        lo, hi = ((0, GU), (GU, ALL))[part]
        return rdma(
            wbuf.at[src, lo:hi, :], wbuf.at[src, lo:hi, :],
            w_send.at[part, i], w_recv.at[part, src], (peer, me),
        )

    def wt_copy(s, i, t):
        return rdma(wt.at[s], wt.at[s], wt_send.at[i], wt_recv.at[s], (f, t))

    def right(t):
        return jnp.minimum(t + 2, T - 2 + lax.rem(t, 2))

    def left(t):
        return jnp.maximum(t - 2, lax.rem(t, 2))

    @pl.when(z < Z - 1)
    def _():
        tok_copy(me, 0, right(me)).start()

    @pl.when(z > 0)
    def _():
        tok_copy(me, 1, left(me)).start()

    tok_copy(me, 2, partner).start()
    for i in range(1, T):
        wt_copy(me, i, lax.rem(me + i, T)).start()
    scale = gain[...]
    wbuf[f, 0:H, :] = (ex_gate[...] * scale).astype(jnp.bfloat16)
    wbuf[f, H:2 * H, :] = (ex_up[...] * scale).astype(jnp.bfloat16)
    wbuf[f, 2 * H:2 * H + S, :] = (sh_gate[...] * scale).astype(jnp.bfloat16)
    wbuf[f, 2 * H + S:GU, :] = (sh_up[...] * scale).astype(jnp.bfloat16)
    wbuf[f, GU:GU + H, :] = ex_down[...].astype(jnp.bfloat16)
    wbuf[f, GU + H:ALL, :] = sh_down[...].astype(jnp.bfloat16)
    for i in range(1, F):
        w_copy(0, f, i, lax.rem(f + i, F)).start()
    for i in range(1, F):
        w_copy(1, f, i, lax.rem(f + i, F)).start()

    def gather_step(k, carry):
        a = me - 2 * k
        b = me + 2 * k

        @pl.when(a >= 0)
        def _():
            tok_copy(a, 0, partner).wait_recv()

            @pl.when(z < Z - 1)
            def _():
                tok_copy(a, 0, right(me)).start()

            tok_copy(a, 2, partner).start()

        @pl.when(b < T)
        def _():
            tok_copy(b, 1, partner).wait_recv()

            @pl.when(z > 0)
            def _():
                tok_copy(b, 1, left(me)).start()

            tok_copy(b, 2, partner).start()

        return carry

    lax.fori_loop(1, Z - 1, gather_step, 0)

    for i in range(1, F):
        w_copy(0, lax.rem(f + F - i, F), i, f).wait_recv()
    for i in range(1, T):
        wt_copy(lax.rem(me + T - i, T), i, me).wait_recv()

    def hidden_step(k, carry):
        tok_copy(2 * k + 1 - c, 0, partner).wait_recv()
        x = tok[pl.ds(2 * k, 2)].reshape(2 * rows, F * cw)
        acc = jnp.zeros((2 * rows, GU), jnp.float32)
        for q in range(F):
            acc = acc + lax.dot_general(
                x[:, q * cw:(q + 1) * cw], wbuf[q, 0:GU, :], CONTRACT,
                preferred_element_type=jnp.float32,
            )
        g, u = acc[:, 0:H], acc[:, H:2 * H]
        sg, su = acc[:, 2 * H:2 * H + S], acc[:, 2 * H + S:GU]
        he = g / (1.0 + jnp.exp(-g)) * u
        hs = sg / (1.0 + jnp.exp(-sg)) * su
        for h in range(2):
            row = wt[2 * k + h, pl.ds(me, 1), :]
            col = jnp.transpose(jnp.broadcast_to(row, (128, rows)))[:, 0:1]
            hid_e[2 * k + h] = (he[h * rows:(h + 1) * rows] * col).astype(jnp.bfloat16)
            hid_s[2 * k + h] = hs[h * rows:(h + 1) * rows].astype(jnp.bfloat16)
        return carry

    def near_step(k, carry):
        @pl.when(jnp.maximum(k - z, z - k) < Z - 1)
        def _():
            hidden_step(k, carry)

        return carry

    lax.fori_loop(0, Z, near_step, 0)
    gather_step(Z - 1, 0)

    @pl.when(z == 0)
    def _():
        hidden_step(Z - 1, 0)

    @pl.when(z == Z - 1)
    def _():
        hidden_step(0, 0)

    ring = pout.shape[0]
    big = Z * F
    near = jnp.minimum(jnp.where(z < Z - 1, z, big), jnp.where(z > 0, Z - 1 - z, big))
    count = Z * (F + Z - 1)

    def unit(n):
        s = n // Z
        i = lax.rem(n, Z)
        d = jnp.where(lax.rem(i, 2) == 0, Z - 1 - i // 2, i // 2)
        away = jnp.where(d > z, z, jnp.where(d < z, Z - 1 - z, jnp.maximum(z, Z - 1 - z)))
        j = s - away
        return j, d, (j >= 0) & (j < F) & (n >= 0) & (n < count)

    def pair_copy(p, slot):
        return rdma(pout.at[p], pin.at[slot], pout_sem.at[p], pin_sem.at[slot], (f, partner))

    def sum_copy(p, slot, t):
        return rdma(sout.at[p], sin.at[slot], sout_sem.at[p], sin_sem.at[slot], (f, t))

    def produce(n, j, d, done):
        q = lax.rem(f + j, F)
        p = lax.rem(done, ring)
        he = hid_e[pl.ds(2 * d, 2)].reshape(2 * rows, H)
        hs = hid_s[pl.ds(2 * d, 2)].reshape(2 * rows, S)
        r = jnp.dot(he, wbuf[q, GU:GU + H, :], preferred_element_type=jnp.float32)
        r = r + jnp.dot(hs, wbuf[q, GU + H:ALL, :], preferred_element_type=jnp.float32)
        top, bottom = r[:rows], r[rows:]
        own[lax.rem(n, LAG + 1)] = jnp.where(c == 0, top, bottom)

        @pl.when(done >= ring)
        def _():
            pair_copy(p, 0).wait_send()

        pout[p] = jnp.where(c == 0, bottom, top).astype(jnp.bfloat16)
        pair_copy(p, j * Z + d).start()

    def finish(n, j, d, sent):
        q = lax.rem(f + j, F)
        o = lax.rem(n, LAG + 1)
        p = lax.rem(sent, ring)
        base = j * (Z + 1)
        pair_copy(0, j * Z + d).wait_recv()
        own[o] = own[o] + pin[j * Z + d].astype(jnp.float32)

        @pl.when((d >= z) & (z > 0))
        def _():
            sum_copy(0, base + d, me).wait_recv()
            own[o] = own[o] + sin[base + d].astype(jnp.float32)

        @pl.when((d <= z) & (z < Z - 1))
        def _():
            slot = base + jnp.where(d == z, Z, d)
            sum_copy(0, slot, me).wait_recv()
            own[o] = own[o] + sin[slot].astype(jnp.float32)

        @pl.when(d != z)
        def _():
            @pl.when(sent >= ring)
            def _():
                sum_copy(p, 0, partner).wait_send()

            sout[p] = own[o].astype(jnp.bfloat16)

            @pl.when(d > z)
            def _():
                sum_copy(p, base + d, right(me)).start()

            @pl.when(d < z)
            def _():
                sum_copy(p, base + jnp.where(d == z - 1, Z, d), left(me)).start()

        @pl.when(d == z)
        def _():
            mix[q] = own[o].astype(jnp.bfloat16)

    def sum_step(n, carry):
        done, sent = carry
        first = n // Z - near

        @pl.when((lax.rem(n, Z) == 0) & (first > 0) & (first < F))
        def _():
            w_copy(1, lax.rem(f + first, F), 1, f).wait_recv()

        j, d, valid = unit(n)

        @pl.when(valid)
        def _():
            produce(n, j, d, done)

        done = done + jnp.where(valid, 1, 0)
        m = n - LAG
        j, d, valid = unit(jnp.maximum(m, 0))
        valid = valid & (m >= 0)

        @pl.when(valid)
        def _():
            finish(m, j, d, sent)

        sent = sent + jnp.where(valid & (d != z), 1, 0)
        return done, sent

    lax.fori_loop(0, count + LAG, sum_step, (0, 0))

    for p in range(ring):
        pair_copy(p, 0).wait_send()
    for p in range(min(ring, (Z - 1) * F)):
        sum_copy(p, 0, partner).wait_send()
    for i in range(1, F):
        w_copy(0, f, i, lax.rem(f + i, F)).wait_send()
        w_copy(1, f, i, lax.rem(f + i, F)).wait_send()
    for i in range(1, T):
        wt_copy(me, i, lax.rem(me + i, T)).wait_send()

    def drain(k, carry):
        s = 2 * k + c

        @pl.when((k <= z) & (z < Z - 1))
        def _():
            tok_copy(s, 0, right(me)).wait_send()

        @pl.when((k >= z) & (z > 0))
        def _():
            tok_copy(s, 1, left(me)).wait_send()

        tok_copy(s, 2, partner).wait_send()
        return carry

    lax.fori_loop(0, Z, drain, 0)


def place(H, S, wbuf, mix, o_mixed, o_eg, o_eu, o_ed, o_sg, o_su, o_sd, sems):
    F, cw = wbuf.shape[0], wbuf.shape[2]
    GU = 2 * H + 2 * S
    pieces = ((o_eg, 0, H), (o_eu, H, H), (o_ed, GU, H), (o_sg, 2 * H, S), (o_su, 2 * H + S, S), (o_sd, GU + H, S))
    copies = []
    for p, (ref, lo, size) in enumerate(pieces):
        for q in range(F):
            copies.append(pltpu.make_async_copy(
                wbuf.at[q, lo:lo + size, :], ref.at[:, q * cw:(q + 1) * cw], sems.at[p, q]
            ))
    for q in range(F):
        copies.append(pltpu.make_async_copy(mix.at[q], o_mixed.at[:, q * cw:(q + 1) * cw], sems.at[6, q]))
    for copy in copies:
        copy.start()
    for copy in copies:
        copy.wait()


def local(F, T, tokens, gain, ex_gate, ex_up, ex_down, sh_gate, sh_up, sh_down, routes, route_weight):
    H, cw = ex_gate.shape[1:]
    S = sh_gate.shape[0]
    M = tokens.shape[0]
    D = tokens.shape[1]
    Z = T // 2
    N, U = (Z - 1) * F, Z * F
    ring = min(U, RING)
    bf, f32 = jnp.bfloat16, jnp.float32
    dma = pltpu.SemaphoreType.DMA
    wbuf, mix = pl.pallas_call(
        functools.partial(kernel, F, T, H, S, M),
        out_shape=[pltpu.VMEM((F, 3 * H + 3 * S, cw), bf), pltpu.VMEM((F, M, cw), bf)],
        in_specs=[pl.BlockSpec(memory_space=pltpu.VMEM)] * 10,
        out_specs=[pl.BlockSpec(memory_space=pltpu.VMEM)] * 2,
        scratch_shapes=[
            pltpu.VMEM((T, M, D), bf),
            pltpu.VMEM((T, T, M), f32),
            pltpu.VMEM((T, M, H), bf),
            pltpu.VMEM((T, M, S), bf),
            pltpu.VMEM((LAG + 1, M, cw), f32),
            pltpu.VMEM((ring, M, cw), bf),
            pltpu.VMEM((U, M, cw), bf),
            pltpu.VMEM((ring, M, cw), bf),
            pltpu.VMEM((F * (Z + 1), M, cw), bf),
            dma((T, 3)),
            dma((T,)),
            dma((T,)),
            dma((T,)),
            dma((2, F)),
            dma((2, F)),
            dma((ring,)),
            dma((U,)),
            dma((ring,)),
            dma((F * (Z + 1),)),
        ],
        compiler_params=pltpu.CompilerParams(
            collective_id=0, has_side_effects=True, vmem_limit_bytes=VMEM_LIMIT
        ),
    )(
        tokens, gain[None, :], ex_gate[0], ex_up[0], ex_down[0], sh_gate, sh_up, sh_down,
        routes.T, route_weight.T,
    )
    mixed, eg, eu, ed, sg, su, sd = pl.pallas_call(
        functools.partial(place, H, S),
        out_shape=[jax.ShapeDtypeStruct((M, D), bf)]
        + [jax.ShapeDtypeStruct((H, D), bf)] * 3
        + [jax.ShapeDtypeStruct((S, D), bf)] * 3,
        in_specs=[pl.BlockSpec(memory_space=pltpu.VMEM)] * 2,
        out_specs=[pl.BlockSpec(memory_space=pl.ANY)] * 7,
        scratch_shapes=[dma((7, F))],
        compiler_params=pltpu.CompilerParams(vmem_limit_bytes=4 << 20),
    )(pltpu.with_memory_space_constraint(wbuf, pltpu.VMEM), pltpu.with_memory_space_constraint(mix, pltpu.VMEM))
    return (mixed, eg[None], eu[None], ed[None], sg, su, sd)


def solution(mesh):
    in_specs = (
        P(("fs", "tp"), None),
        P("fs"),
        P("tp", None, "fs"),
        P("tp", None, "fs"),
        P("tp", None, "fs"),
        P("tp", "fs"),
        P("tp", "fs"),
        P("tp", "fs"),
        P(("fs", "tp"), None),
        P(("fs", "tp"), None),
    )
    out_specs = (
        P(("fs", "tp"), None),
        P("tp", None, None),
        P("tp", None, None),
        P("tp", None, None),
        P("tp", None),
        P("tp", None),
        P("tp", None),
    )
    step = functools.partial(local, mesh.shape["fs"], mesh.shape["tp"])
    return jax.shard_map(step, mesh=mesh, in_specs=in_specs, out_specs=out_specs, check_vma=False)
```

time: 115 us -> 93.3 us (0.81)
  local copies, waits for them, and re-layouts: 11.2 us -> 0 us
  Pallas kernels: 102 us -> 92.5 us
    unnamed x25 -> x0, local copies, waits for them, and re-layouts: 11.2 us -> none
    pallas_call x1 -> x2, Pallas kernels: 102 us -> 92.5 us  [the longest x1 90.2 us: local(): pl.pallas_call(functools.partial(kernel, F, T, H, S, M), out_shape=[pltpu...]
where the time goes in v2:
time: 93.3 us; the launch traced here: 93.1 us
  Pallas kernels  92.5 us (99%)
    pallas_call x1, Pallas kernels, local(): pl.pallas_call(functools.partial(kernel, F, T, H, S, M), out_shape=[pltpu...  90.2 us
    pallas_call x1, Pallas kernels, local(): pl.pallas_call(functools.partial(place, H, S), out_shape=[jax.ShapeDtypeS...  2.32 us

profile of v2, /device:TPU:0, one launch (start us, length us, event | category | flops | bytes accessed | tf_op | source)
XLA Modules:
  0.0 93.1 jit_solution(14656286202116292073)
XLA Ops:
  0.6 90.2 %shard_map.153 = (bf16[4,960,512]{2,1,0:T(8,128)(2,1)S(1)}, bf16[4,128,512]{2,1,0:T(8,128)(2,1)S(1)}) custom-call(bf16[128,2048]{1,0:T(8,128)(2,1)} %tokens.1, f32[1,512]{1,0:T(1,128)} %bitcast.12, f32[256,512]{1,0:T(8,128)} %bitcast.9, f32[256,512]{1,0:T(8,128)} %bitcast.10, f32[256,512]{1,0:T(8,128)} %bitcast.11, f32[64,512]{1,0:T(8,128)} %sh_gate.1, ...), custom_call_target="tpu_custom_call" | custom-call | tf_op jit(solution)/shard_map/pallas_call | solution.py:335
  90.8 2.3 %shard_map.154 = (bf16[128,2048]{1,0:T(8,128)(2,1)}, bf16[256,2048]{1,0:T(8,128)(2,1)}, bf16[256,2048]{1,0:T(8,128)(2,1)}, bf16[256,2048]{1,0:T(8,128)(2,1)}, bf...) custom-call(bf16[4,960,512]{2,1,0:T(8,128)(2,1)S(1)} %get-tuple-element.16.wbuf, ...), custom_call_target="tpu_custom_call" | custom-call | tf_op jit(solution)/shard_map/pallas_call | solution.py:368

commit v3 on v2

--- a/solution.py
+++ b/solution.py
@@ -23,6 +23,7 @@
     tok, wt, hid_e, hid_s, own, pout, pin, sout, sin,
     ag_send, ag_recv, wt_send, wt_recv, w_send, w_recv,
     pout_sem, pin_sem, sout_sem, sin_sem,
+    l_eg, l_eu, l_ed, l_sg, l_su, l_sd, load_sem,
 ):
     f = lax.axis_index("fs")
     me = lax.axis_index("tp")
@@ -35,6 +36,14 @@
     ALL = 3 * H + 3 * S
     partner = 2 * z + 1 - c
 
+    loads = [
+        pltpu.make_async_copy(src, dst, load_sem.at[i])
+        for i, (src, dst) in enumerate((
+            (ex_gate, l_eg), (ex_up, l_eu), (sh_gate, l_sg), (sh_up, l_su), (ex_down, l_ed), (sh_down, l_sd)
+        ))
+    ]
+    for load in loads:
+        load.start()
     barrier = pltpu.get_barrier_semaphore()
     for i in range(1, F):
         pl.semaphore_signal(barrier, inc=1, device_id=(lax.rem(f + i, F), me), device_id_type=MESH)
@@ -91,13 +100,15 @@
     tok_copy(me, 2, partner).start()
     for i in range(1, T):
         wt_copy(me, i, lax.rem(me + i, T)).start()
+    for load in loads:
+        load.wait()
     scale = gain[...]
-    wbuf[f, 0:H, :] = (ex_gate[...] * scale).astype(jnp.bfloat16)
-    wbuf[f, H:2 * H, :] = (ex_up[...] * scale).astype(jnp.bfloat16)
-    wbuf[f, 2 * H:2 * H + S, :] = (sh_gate[...] * scale).astype(jnp.bfloat16)
-    wbuf[f, 2 * H + S:GU, :] = (sh_up[...] * scale).astype(jnp.bfloat16)
-    wbuf[f, GU:GU + H, :] = ex_down[...].astype(jnp.bfloat16)
-    wbuf[f, GU + H:ALL, :] = sh_down[...].astype(jnp.bfloat16)
+    wbuf[f, 0:H, :] = (l_eg[...] * scale).astype(jnp.bfloat16)
+    wbuf[f, H:2 * H, :] = (l_eu[...] * scale).astype(jnp.bfloat16)
+    wbuf[f, 2 * H:2 * H + S, :] = (l_sg[...] * scale).astype(jnp.bfloat16)
+    wbuf[f, 2 * H + S:GU, :] = (l_su[...] * scale).astype(jnp.bfloat16)
+    wbuf[f, GU:GU + H, :] = l_ed[...].astype(jnp.bfloat16)
+    wbuf[f, GU + H:ALL, :] = l_sd[...].astype(jnp.bfloat16)
     for i in range(1, F):
         w_copy(0, f, i, lax.rem(f + i, F)).start()
     for i in range(1, F):
@@ -182,7 +193,9 @@
     def unit(n):
         s = n // Z
         i = lax.rem(n, Z)
-        d = jnp.where(lax.rem(i, 2) == 0, Z - 1 - i // 2, i // 2)
+        left_half = 2 * z < Z
+        i = jnp.where(i == Z - 1, -1, i + jnp.where(i >= jnp.where(left_half, Z - 1 - z, z), 1, 0))
+        d = jnp.where(i < 0, z, jnp.where(left_half, Z - 1 - i, i))
         away = jnp.where(d > z, z, jnp.where(d < z, Z - 1 - z, jnp.maximum(z, Z - 1 - z)))
         j = s - away
         return j, d, (j >= 0) & (j < F) & (n >= 0) & (n < count)
@@ -335,7 +348,9 @@
     wbuf, mix = pl.pallas_call(
         functools.partial(kernel, F, T, H, S, M),
         out_shape=[pltpu.VMEM((F, 3 * H + 3 * S, cw), bf), pltpu.VMEM((F, M, cw), bf)],
-        in_specs=[pl.BlockSpec(memory_space=pltpu.VMEM)] * 10,
+        in_specs=[pl.BlockSpec(memory_space=pltpu.VMEM)] * 2
+        + [pl.BlockSpec(memory_space=pl.ANY)] * 6
+        + [pl.BlockSpec(memory_space=pltpu.VMEM)] * 2,
         out_specs=[pl.BlockSpec(memory_space=pltpu.VMEM)] * 2,
         scratch_shapes=[
             pltpu.VMEM((T, M, D), bf),
@@ -357,6 +372,13 @@
             dma((U,)),
             dma((ring,)),
             dma((F * (Z + 1),)),
+            pltpu.VMEM((H, cw), f32),
+            pltpu.VMEM((H, cw), f32),
+            pltpu.VMEM((H, cw), f32),
+            pltpu.VMEM((S, cw), f32),
+            pltpu.VMEM((S, cw), f32),
+            pltpu.VMEM((S, cw), f32),
+            dma((6,)),
         ],
         compiler_params=pltpu.CompilerParams(
             collective_id=0, has_side_effects=True, vmem_limit_bytes=VMEM_LIMIT

time: 93.3 us -> 92.3 us (0.989)
  Pallas kernels: 92.5 us -> 91.5 us
    pallas_call x1, Pallas kernels: 90.2 us -> 89.2 us  [local(): pl.pallas_call(functools.partial(kernel, F, T, H, S, M), out_shape=[pltpu...]
where the time goes in v3:
time: 92.3 us; the launch traced here: 92.2 us
  Pallas kernels  91.5 us (99%)
    pallas_call x1, Pallas kernels, local(): pl.pallas_call(functools.partial(kernel, F, T, H, S, M), out_shape=[pltpu...  89.2 us
    pallas_call x1, Pallas kernels, local(): pl.pallas_call(functools.partial(place, H, S), out_shape=[jax.ShapeDtypeS...  2.32 us

profile of v3, /device:TPU:0, one launch (start us, length us, event | category | flops | bytes accessed | tf_op | source)
XLA Modules:
  0.0 92.2 jit_solution(3725099365493831949)
XLA Ops:
  0.6 89.2 %shard_map.153 = (bf16[4,960,512]{2,1,0:T(8,128)(2,1)S(1)}, bf16[4,128,512]{2,1,0:T(8,128)(2,1)S(1)}) custom-call(bf16[128,2048]{1,0:T(8,128)(2,1)} %tokens.1, f32[1,512]{1,0:T(1,128)} %bitcast.12, f32[256,512]{1,0:T(8,128)} %bitcast.9, f32[256,512]{1,0:T(8,128)} %bitcast.10, f32[256,512]{1,0:T(8,128)} %bitcast.11, f32[64,512]{1,0:T(8,128)} %sh_gate.1, ...), custom_call_target="tpu_custom_call" | custom-call | tf_op jit(solution)/shard_map/pallas_call | solution.py:348
  89.9 2.3 %shard_map.154 = (bf16[128,2048]{1,0:T(8,128)(2,1)}, bf16[256,2048]{1,0:T(8,128)(2,1)}, bf16[256,2048]{1,0:T(8,128)(2,1)}, bf16[256,2048]{1,0:T(8,128)(2,1)}, bf...) custom-call(bf16[4,960,512]{2,1,0:T(8,128)(2,1)S(1)} %get-tuple-element.16.wbuf, ...), custom_call_target="tpu_custom_call" | custom-call | tf_op jit(solution)/shard_map/pallas_call | solution.py:390
